TPU v7x, 256 devices: a whole 4x4x8 slice. The times are simulated.
256 devices in a mesh: kv: 16 (over y, x), tp: 16 (over z, core).
Axes of the slice: x: 4, y: 4, z: 8, core: 2. Of those that a mesh axis runs over, the one named last changes fastest.
Arguments:
- tokens: bfloat16 [128, 4096], P(None, ('kv', 'tp')), may hold values from -41 to 41
- lengths: int32 [128], P('kv'), may hold values from 1 to 8192, 262144 in all
- retention_state: float32 [128, 16, 128, 256], P('kv', 'tp'), may hold values from -4 to 4
- mixer_gain: float32 [4096], P('kv'), may hold values from 0.1 to 1.9
- query_weight: bfloat16 [4096, 2048], P('kv', 'tp'), may hold values from -0.09375 to 0.09375
- key_weight: bfloat16 [4096, 2048], P('kv', 'tp'), may hold values from -0.09375 to 0.09375
- value_weight: bfloat16 [4096, 4096], P('kv', 'tp'), may hold values from -0.09375 to 0.09375
- gate_weight: bfloat16 [4096, 4096], P('kv', 'tp'), may hold values from -0.09375 to 0.09375
- output_weight: bfloat16 [4096, 4096], P('tp', 'kv'), may hold values from -0.125 to 0.125
- channel_gain: float32 [4096], P('kv'), may hold values from 0.1 to 1.9
- ffn_gate: bfloat16 [4096, 11264], P('kv', 'tp'), may hold values from -0.09375 to 0.09375
- ffn_up: bfloat16 [4096, 11264], P('kv', 'tp'), may hold values from -0.09375 to 0.09375
- ffn_down: bfloat16 [11264, 4096], P('tp', 'kv'), may hold values from -0.078125 to 0.078125
Outputs:
- layer_output: bfloat16 [128, 4096], P(None, ('kv', 'tp'))
- new_state: float32 [128, 16, 128, 256], P('kv', 'tp')
All inputs are finite; a program needn't handle non-finite values. No bound on the sum of `lengths` on one device may be relied on, other than what follows from the above.
Results may differ from a plain program's by a relative error of at most 0.022.
Values may be sent and summed in bfloat16 or wider, within the bound.
A program may use at most 64 MiB of HBM per device.

v0:
```python
import jax
import jax.numpy as jnp
from jax import lax
from jax.sharding import PartitionSpec as P

D = 4096
HEADS = 16
QK = 128


def in_blocks(value, dim, devices):
    lengths = value.shape
    blocks = value.reshape(*lengths[:dim], devices, lengths[dim] // devices, *lengths[dim + 1 :])
    return jnp.moveaxis(blocks, dim, 0)


def sent_and_summed(value, axis, dim):
    blocks = in_blocks(value, dim, lax.axis_size(axis))
    arrived = lax.all_to_all(blocks, axis, split_axis=0, concat_axis=0, tiled=True)
    return arrived.astype(jnp.float32).sum(axis=0)


def in_one_piece(arrays, axis, dim, along):
    columns = [a.reshape(*a.shape[:along], -1) for a in arrays]
    both = jnp.concatenate(columns, axis=along)
    result, at, finished = (sent_and_summed(both, axis, dim), 0, [])
    for a, column in zip(arrays, columns):
        piece = result[..., at : at + column.shape[along]]
        finished.append(piece.reshape(*piece.shape[:along], *a.shape[along:]))
        at += column.shape[along]
    return tuple(finished)


def copy_for_each(value, axis):
    devices = lax.axis_size(axis)
    return lax.all_to_all(
        jnp.broadcast_to(value[None], (devices, *value.shape)), axis, 0, 0, tiled=True
    )


def joined_along(blocks, dim):
    blocks = jnp.moveaxis(blocks, 0, dim)
    lengths = blocks.shape
    return blocks.reshape(*lengths[:dim], lengths[dim] * lengths[dim + 1], *lengths[dim + 2 :])


def gather_directly(value, axis, dim):
    blocks = copy_for_each(value, axis)
    return joined_along(blocks, dim)


def rotate_heads(vectors, positions):
    half_dim = vectors.shape[-1] // 2
    frequency = 10000.0 ** (-jnp.arange(half_dim, dtype=jnp.float32) / half_dim)
    angles = positions.astype(jnp.float32)[:, None, None] * frequency
    cosine = jnp.cos(angles)
    sine_part = jnp.sin(angles)
    first_half = vectors[..., :half_dim]
    second = vectors[..., half_dim:]
    return jnp.concatenate(
        [first_half * cosine - second * sine_part, first_half * sine_part + second * cosine],
        axis=-1,
    )


def gathered_rows(columns):
    return lax.all_gather(columns, "tp", axis=1, tiled=True)


def owned_sums(partial_value, squares):
    raw_sums, totals = in_one_piece(
        (partial_value.astype(jnp.bfloat16), squares.astype(jnp.bfloat16)), "kv", 0, 1
    )
    summed = raw_sums * lax.rsqrt(totals / D + 1e-06)[:, None]
    return summed


def on_device(
    tokens,
    lengths,
    retention_state,
    mixer_gain,
    query_weight,
    key_weight,
    value_weight,
    gate_weight,
    output_weight,
    channel_gain,
    ffn_gate,
    ffn_up,
    ffn_down,
):
    feature_block = gathered_rows(tokens).astype(jnp.float32)
    squares = jnp.sum(feature_block * feature_block, axis=1)
    normed = (feature_block * mixer_gain).astype(jnp.bfloat16)
    partial_value = jnp.concatenate(
        [
            jnp.dot(normed, query_weight, preferred_element_type=jnp.float32),
            jnp.dot(normed, key_weight, preferred_element_type=jnp.float32),
            jnp.dot(normed, value_weight, preferred_element_type=jnp.float32),
            jnp.dot(normed, gate_weight, preferred_element_type=jnp.float32),
        ],
        axis=1,
    )
    owned_rows = owned_sums(partial_value, squares)
    local_heads = query_weight.shape[1] // QK
    q_width = query_weight.shape[1]
    v_width = value_weight.shape[1]
    head_width = v_width // local_heads
    seq_rows = owned_rows.shape[0]
    query_rows = rotate_heads(
        owned_rows[:, :q_width].reshape(seq_rows, local_heads, QK), lengths
    ).astype(jnp.bfloat16)
    key_rows = (
        rotate_heads(
            owned_rows[:, q_width : 2 * q_width].reshape(seq_rows, local_heads, QK), lengths
        )
        * QK ** (-0.5)
    ).astype(jnp.bfloat16)
    value_rows = (
        owned_rows[:, 2 * q_width : 2 * q_width + v_width]
        .astype(jnp.bfloat16)
        .reshape(seq_rows, local_heads, head_width)
    )
    gate_rows = owned_rows[:, 2 * q_width + v_width :]
    head_ids = (lax.axis_index("tp") * local_heads + jnp.arange(local_heads)).astype(jnp.float32)
    decay_rate = 1.0 - 2.0 ** (-5.0 - 10.0 * head_ids / (HEADS - 1))
    new_state = (
        decay_rate[None, :, None, None] * retention_state
        + key_rows.astype(jnp.float32)[..., :, None] * value_rows.astype(jnp.float32)[..., None, :]
    )
    retained = jnp.einsum(
        "bhk,bhkv->bhv", query_rows.astype(jnp.float32), new_state, precision=lax.Precision.HIGHEST
    )
    normalized = retained * lax.rsqrt(jnp.mean(retained * retained, axis=-1) + 1e-06)[..., None]
    merged = (normalized.reshape(seq_rows, v_width) * jax.nn.silu(gate_rows)).astype(jnp.bfloat16)
    mixed_part = jnp.dot(
        gather_directly(merged, "kv", 0), output_weight, preferred_element_type=jnp.float32
    )
    mixed_cols = sent_and_summed(mixed_part.astype(jnp.bfloat16), "tp", 1)
    residual = (tokens.astype(jnp.float32) + mixed_cols).astype(jnp.bfloat16)
    block_two = gathered_rows(residual).astype(jnp.float32)
    squares_two = jnp.sum(block_two * block_two, axis=1)
    normed_two = (block_two * channel_gain).astype(jnp.bfloat16)
    partial_two = jnp.concatenate(
        [
            jnp.dot(normed_two, ffn_gate, preferred_element_type=jnp.float32),
            jnp.dot(normed_two, ffn_up, preferred_element_type=jnp.float32),
        ],
        axis=1,
    )
    hidden_units = ffn_gate.shape[1]
    summed = owned_sums(partial_two, squares_two)
    hidden = (jax.nn.silu(summed[:, :hidden_units]) * summed[:, hidden_units:]).astype(jnp.bfloat16)
    down_part = jnp.dot(
        gather_directly(hidden, "kv", 0), ffn_down, preferred_element_type=jnp.float32
    )
    down_sums = sent_and_summed(down_part.astype(jnp.bfloat16), "tp", 1)
    layer_output = (residual.astype(jnp.float32) + down_sums).astype(jnp.bfloat16)
    return (layer_output, new_state)


def solution(mesh):
    in_specs = (
        P(None, ("kv", "tp")),
        P("kv"),
        P("kv", "tp", None, None),
        P("kv"),
        P("kv", "tp"),
        P("kv", "tp"),
        P("kv", "tp"),
        P("kv", "tp"),
        P("tp", "kv"),
        P("kv"),
        P("kv", "tp"),
        P("kv", "tp"),
        P("tp", "kv"),
    )
    out_specs = (P(None, ("kv", "tp")), P("kv", "tp", None, None))
    return jax.shard_map(
        on_device, mesh=mesh, in_specs=in_specs, out_specs=out_specs, check_vma=False
    )
```

profile of v0, /device:TPU:1, one launch (start us, length us, event | category | flops | bytes accessed | tf_op | source)
XLA Modules:
  0.0 126.4 jit_solution(4354620266394448964)
XLA Ops:
  0.6 0.0 copy-start
  0.6 0.0 copy-start.2
  0.7 21.8 %all_gather.6 = bf16[128,256]{0,1:T(8,128)(2,1)S(1)} all-gather(bf16[128,16]{0,1:T(8,128)(2,1)} %param.13), channel_id=1, replica_groups=mesh['kv'=16,'tp'=16] {'tp'}, dimensions={1}, use_global_device_ids=true | all-gather | bytes 69632 | tf_op jit(solution)/shard_map/all_gather | solution.py:67
  22.5 0.1 fusion.12
  22.6 0.2 convert_element_type.141
  22.8 1.8 %fusion.5 = bf16[16,8,769]{2,1,0:T(8,128)(2,1)} fusion(bf16[256,128]{1,0:T(8,128)(2,1)} %param.17, bf16[128,256]{0,1:T(8,128)(2,1)S(1)} %all_gather.6, f32[256]{0:T(256)} %param.16), kind=kOutput, calls=%fused_computation.13 | convolution fusion | flops 8503295 | bytes 164864 | tf_op jit(solution)/shard_map/dot_general | solution.py:98
  24.6 1.8 %fusion.7 = bf16[16,8,769]{2,1,0:T(8,128)(2,1)} fusion(bf16[16,8,769]{2,1,0:T(8,128)(2,1)} %fusion.5, bf16[256,128]{1,0:T(8,128)(2,1)} %param.18, bf16[128,256]{0,1:T(8,128)(2,1)S(1)} %all_gather.6, f32[256]{0:T(256)} %param.16), kind=kOutput, calls=%fused_computation.15 | convolution fusion | flops 8503296 | bytes 164864 | tf_op jit(solution)/shard_map/dot_general | solution.py:99
  26.3 1.8 %fusion.1 = bf16[16,8,769]{2,1,0:T(8,128)(2,1)} fusion(bf16[16,8,769]{2,1,0:T(8,128)(2,1)} %fusion.7, bf16[256,256]{1,0:T(8,128)(2,1)} %param.19, bf16[128,256]{0,1:T(8,128)(2,1)S(1)} %all_gather.6, f32[256]{0:T(256)} %param.16), kind=kOutput, calls=%fused_computation.7 | convolution fusion | flops 16908288 | bytes 263168 | tf_op jit(solution)/shard_map/dot_general | solution.py:100
  28.1 1.8 %fusion.3 = bf16[16,8,769]{2,1,0:T(8,128)(2,1)} fusion(bf16[16,8,769]{2,1,0:T(8,128)(2,1)} %fusion.1, bf16[256,256]{1,0:T(8,128)(2,1)} %param.20, bf16[128,256]{0,1:T(8,128)(2,1)S(1)} %all_gather.6, f32[256]{0:T(256)} %param.16), kind=kOutput, calls=%fused_computation.9 | convolution fusion | flops 16908288 | bytes 263168 | tf_op jit(solution)/shard_map/dot_general | solution.py:101
  30.0 0.6 constant_dynamic-update-slice_fusion
  30.6 6.8 %all-to-all-start = ((bf16[16,8,769]{2,1,0:T(8,128)(2,1)}), bf16[16,8,769]{2,1,0:T(8,128)(2,1)S(1)}, u32[]{:S(2)}, u32[]{:S(2)}) async-start(bf16[16,8,769]{2,1,0:T(8,128)(2,1)} %constant_dynamic-update-slice_fusion), calls=%async_computation | async-start | bytes 458752 | tf_op jit(solution)/shard_map/all_to_all | solution.py:19
  37.4 0.0 copy-start.8
  37.4 0.6 copy-done.8
  38.1 7.3 %all-to-all-done = bf16[16,8,769]{2,1,0:T(8,128)(2,1)S(1)} async-done(((bf16[16,8,769]{2,1,0:T(8,128)(2,1)}), bf16[16,8,769]{2,1,0:T(8,128)(2,1)S(1)}, u32[]{:S(2)}, u32[]{:S(2)}) %all-to-all-start) | async-done | bytes 196896 | tf_op jit(solution)/shard_map/all_to_all | solution.py:19
  45.4 0.1 fusion.44
  45.5 0.1 slice_multiply_fusion.2
  45.6 0.1 fusion.49
  45.7 0.1 maximum_bitcast_fusion
  45.8 0.1 fusion.47
  45.9 0.0 copy-done.2
  45.9 0.2 multiply_add_fusion
  46.1 0.0 copy-start.1
  46.1 0.5 fusion.8
  46.6 0.0 copy-start.5
  46.6 0.1 fusion.19
  46.7 0.1 fusion.21
  46.8 9.2 %all_to_all.30 = bf16[16,8,256]{2,1,0:T(8,128)(2,1)S(1)} all-to-all(bf16[16,8,256]{2,1,0:T(8,128)(2,1)S(1)} %broadcast_in_dim.4), channel_id=1, replica_groups=mesh['kv'=16,'tp'=16] {'kv'}, dimensions={0} | all-to-all | bytes 131072 | tf_op jit(solution)/shard_map/all_to_all | solution.py:36
  55.9 0.0 copy-done.5
  56.0 0.2 convolution_convert_fusion.3
  56.1 0.1 copy.37
  56.2 13.9 %all_to_all.31 = bf16[16,128,16]{1,2,0:T(8,128)(2,1)S(1)} all-to-all(bf16[16,128,16]{1,2,0:T(8,128)(2,1)S(1)} %bitcast.66), channel_id=1, replica_groups=mesh['kv'=16,'tp'=16] {'tp'}, dimensions={0} | all-to-all | bytes 131072 | tf_op jit(solution)/shard_map/all_to_all | solution.py:19
  70.2 0.0 copy-start.6
  70.2 0.7 copy-done.6
  70.9 14.9 %all_gather.7 = bf16[128,256]{0,1:T(8,128)(2,1)S(1)} all-gather(bf16[128,16]{0,1:T(8,128)(2,1)S(1)} %add_convert_fusion.1), channel_id=1, replica_groups=mesh['kv'=16,'tp'=16] {'tp'}, dimensions={1}, use_global_device_ids=true | all-gather | bytes 69632 | tf_op jit(solution)/shard_map/all_gather | solution.py:67
  85.7 0.1 fusion.14
  85.8 0.0 copy-start.7
  85.8 0.2 convert_element_type.142
  86.0 0.0 copy-done
  86.0 0.4 copy-done.7
  86.5 0.0 copy-start.3
  86.5 0.3 convolution_convert_fusion.1
  86.8 0.0 copy-done.1
  86.8 0.1 copy.38
  86.9 0.5 copy-done.3
  87.4 0.3 convolution_convert_fusion
  87.8 0.1 copy.39
  87.9 0.2 concatenate.65
  88.1 12.3 %all_to_all.32 = bf16[16,8,1409]{2,1,0:T(8,128)(2,1)S(1)} all-to-all(bf16[16,8,1409]{2,1,0:T(8,128)(2,1)S(1)} %concatenate.65), channel_id=1, replica_groups=mesh['kv'=16,'tp'=16] {'kv'}, dimensions={0} | all-to-all | bytes 721408 | tf_op jit(solution)/shard_map/all_to_all | solution.py:19
  100.4 0.1 convert_reduce_fusion
  100.5 0.1 fusion.41
  100.6 0.0 copy-start.4
  100.6 0.1 slice_multiply_fusion
  100.7 0.1 fusion.18
  100.8 10.4 %all_to_all.33 = bf16[16,8,704]{2,1,0:T(8,128)(2,1)S(1)} all-to-all(bf16[16,8,704]{2,1,0:T(8,128)(2,1)S(1)} %broadcast_in_dim.5), channel_id=1, replica_groups=mesh['kv'=16,'tp'=16] {'kv'}, dimensions={0} | all-to-all | bytes 360448 | tf_op jit(solution)/shard_map/all_to_all | solution.py:36
  111.1 0.0 copy-done.4
  111.1 0.2 convolution_convert_fusion.2
  111.4 0.1 copy.41
  111.5 14.3 %all_to_all.34 = bf16[16,128,16]{1,2,0:T(8,128)(2,1)S(1)} all-to-all(bf16[16,128,16]{1,2,0:T(8,128)(2,1)S(1)} %bitcast.67), channel_id=1, replica_groups=mesh['kv'=16,'tp'=16] {'tp'}, dimensions={0} | all-to-all | bytes 131072 | tf_op jit(solution)/shard_map/all_to_all | solution.py:19
  125.8 0.6 add_convert_fusion
  (11 shorter events, 0.1 us)
Async XLA Ops:
  0.6 85.4 %copy-start = (bf16[256,704]{0,1:T(8,128)(2,1)S(1)}, bf16[256,704]{0,1:T(8,128)(2,1)}, u32[]{:S(2)}) copy-start(bf16[256,704]{0,1:T(8,128)(2,1)} %param.23) | copy-start | bytes 1081348
  0.6 45.2 %copy-start.2 = (f32[8,1,128,256]{3,2,1,0:T(8,128)S(1)}, f32[8,1,128,256]{3,2,1,0:T(8,128)}, u32[]{:S(2)}) copy-start(f32[8,1,128,256]{3,2,1,0:T(8,128)} %param.15) | copy-start | bytes 3145732
  30.6 14.7 %all-to-all-start = ((bf16[16,8,769]{2,1,0:T(8,128)(2,1)}), bf16[16,8,769]{2,1,0:T(8,128)(2,1)S(1)}, u32[]{:S(2)}, u32[]{:S(2)}) async-start(bf16[16,8,769]{2,1,0:T(8,128)(2,1)} %constant_dynamic-update-slice_fusion), calls=%async_computation | async-start | bytes 458752 | tf_op jit(solution)/shard_map/all_to_all | solution.py:19
  37.4 0.7 copy-start.8
  46.1 40.7 %copy-start.1 = (f32[8,1,128,256]{3,2,1,0:T(8,128)}, f32[8,1,128,256]{3,2,1,0:T(8,128)S(1)}, u32[]{:S(2)}) copy-start(f32[8,1,128,256]{3,2,1,0:T(8,128)S(1)} %multiply_add_fusion) | copy-start | bytes 3145732
  46.6 9.4 %copy-start.5 = (bf16[256,256]{1,0:T(8,128)(2,1)S(1)}, bf16[256,256]{1,0:T(8,128)(2,1)}, u32[]{:S(2)}) copy-start(bf16[256,256]{1,0:T(8,128)(2,1)} %param.21) | copy-start | bytes 393220
  70.2 0.7 copy-start.6
  85.8 0.7 copy-start.7
  86.5 1.0 copy-start.3
  100.6 10.6 %copy-start.4 = (bf16[704,256]{1,0:T(8,128)(2,1)S(1)}, bf16[704,256]{1,0:T(8,128)(2,1)}, u32[]{:S(2)}) copy-start(bf16[704,256]{1,0:T(8,128)(2,1)} %param.25) | copy-start | bytes 1081348
where the time goes:
time: 127 us; the launch traced here: 126 us
  blocking collectives  96.8 us (76%)
  matrix products  8.66 us (7%)
  waiting for transfers between devices  7.25 us (6%)
  starting transfers between devices  6.75 us (5%)
  local copies, waits for them, and re-layouts  4.08 us (3%)
  other arithmetic  1.99 us (2%)
    all_to_all x3, blocking collectives, sent_and_summed(): lax.all_to_all(blocks, axis, split_axis=0, concat_axis=0, tiled=True)  40.5 us
    all_gather x2, blocking collectives, gathered_rows(): return lax.all_gather(columns, 'tp', axis=1, tiled=True)  36.7 us
    all_to_all x2, blocking collectives, copy_for_each(): lax.all_to_all(jnp.broadcast_to(value[None], (devices, *value.shape)), ax...  19.6 us
    all_to_all x1, waiting for transfers between devices, sent_and_summed(): lax.all_to_all(blocks, axis, split_axis=0, concat_axis=0, tiled=True)  7.25 us
    all_to_all x1, starting transfers between devices, sent_and_summed(): lax.all_to_all(blocks, axis, split_axis=0, concat_axis=0, tiled=True)  6.75 us
  transfers between devices with their start and end apart: 1, of which 1 were waited for; matrix products, arithmetic and copies ran while one was open for 0% of the time, Pallas kernels for 0%

commit v1 on v0

v1 whole, which is shorter than its diff:
```python
import functools

import jax
import jax.numpy as jnp
from jax import lax
from jax.experimental import pallas as pl
from jax.experimental.pallas import tpu as pltpu
from jax.sharding import PartitionSpec as P

D = 4096
HEADS = 16
QK = 128
VD = 256
BATCH = 128
F32 = jnp.float32
BF16 = jnp.bfloat16


def ring_distance(offset, size):
    return min(offset, size - offset)


KV_OFFSETS = sorted(
    [(dy, dx) for dy in range(4) for dx in range(4) if (dy, dx) != (0, 0)],
    key=lambda o: -(ring_distance(o[0], 4) + ring_distance(o[1], 4)),
)
TP_OFFSETS = sorted(
    [(dz, dc) for dz in range(8) for dc in range(2) if (dz, dc) != (0, 0)],
    key=lambda o: -(2 * ring_distance(o[0], 8) + o[1]),
)
N_WEIGHT_COPIES = 12
(TOK, SQ1, QKVG, MERGED, MIXED, RESID, SQ2, FFN, HIDDEN, DOWN) = range(10)


def kernel(
    tokens_hbm,
    lengths,
    state_hbm,
    gain1_hbm,
    wq_hbm,
    wk_hbm,
    wv_hbm,
    wg_hbm,
    wo_hbm,
    gain2_hbm,
    fg_hbm,
    fu_hbm,
    fd_hbm,
    out_ref,
    new_state_hbm,
    tok_own,
    gain1,
    gain2,
    w_in,
    w_out,
    w_out_t,
    w_ff,
    w_down,
    w_down_t,
    state,
    new_state,
    tok_all,
    sq_own,
    sq_all,
    proj_own,
    proj_all,
    merged_own,
    merged_all,
    mixed_own,
    mixed_all,
    resid_own,
    resid_all,
    sq2_own,
    sq2_all,
    ffn_own,
    ffn_all,
    hidden_own,
    hidden_all,
    down_own,
    down_all,
    load_sem,
    store_sem,
    send_sem,
    recv_sem,
):
    kv = lax.axis_index("kv")
    tp = lax.axis_index("tp")
    ky, kx = kv // 4, kv % 4
    tz, tc = tp // 2, tp % 2
    kv_peers = [lax.rem(ky + dy, 4) * 4 + lax.rem(kx + dx, 4) for dy, dx in KV_OFFSETS]
    tp_peers = [
        lax.rem(tz + dz, 8) * 2 + (lax.rem(tc + dc, 2)) for dz, dc in TP_OFFSETS
    ]

    loads = {}
    for number, (name, source, target) in enumerate(
        [
            ("tok", tokens_hbm, tok_own),
            ("gain1", gain1_hbm, gain1),
            ("wq", wq_hbm, w_in.at[:, pl.ds(0, 128)]),
            ("wk", wk_hbm, w_in.at[:, pl.ds(128, 128)]),
            ("wv", wv_hbm, w_in.at[:, pl.ds(256, 256)]),
            ("wg", wg_hbm, w_in.at[:, pl.ds(512, 256)]),
            ("state", state_hbm, state),
            ("wo", wo_hbm, w_out),
            ("gain2", gain2_hbm, gain2),
            ("fg", fg_hbm, w_ff.at[pl.ds(0, 704), :]),
            ("fu", fu_hbm, w_ff.at[pl.ds(704, 704), :]),
            ("fd", fd_hbm, w_down),
        ]
    ):
        copy = pltpu.make_async_copy(source, target, load_sem.at[number])
        copy.start()
        loads[name] = copy

    barrier = pltpu.get_barrier_semaphore()
    for peer in tp_peers:
        pl.semaphore_signal(barrier, inc=1, device_id={"tp": peer}, device_id_type=pl.DeviceIdType.MESH)
    for peer in kv_peers:
        pl.semaphore_signal(barrier, inc=1, device_id={"kv": peer}, device_id_type=pl.DeviceIdType.MESH)

    def exchange(phase, axis, source_for, target):
        me, peers = (kv, kv_peers) if axis == "kv" else (tp, tp_peers)
        sends = []
        for peer in peers:
            copy = pltpu.make_async_remote_copy(
                src_ref=source_for(peer),
                dst_ref=target.at[me],
                send_sem=send_sem.at[phase, peer],
                recv_sem=recv_sem.at[phase, me],
                device_id={axis: peer},
                device_id_type=pl.DeviceIdType.MESH,
            )
            copy.start()
            sends.append(copy)

        def wait_recv():
            for peer in reversed(peers):
                pltpu.make_async_remote_copy(
                    src_ref=source_for(peer),
                    dst_ref=target.at[peer],
                    send_sem=send_sem.at[phase, peer],
                    recv_sem=recv_sem.at[phase, peer],
                    device_id={axis: peer},
                    device_id_type=pl.DeviceIdType.MESH,
                ).wait_recv()

        def wait_send():
            for copy in sends:
                copy.wait_send()

        pending.append(wait_send)
        return wait_recv

    pending = []

    lane = lax.broadcasted_iota(jnp.int32, (8, 128), 1) % 64
    row = lax.broadcasted_iota(jnp.int32, (8, 128), 0)
    frequency = jnp.ones((8, 128), F32)
    for bit in range(6):
        factor = 10000.0 ** (-(2.0**bit) / 64.0)
        frequency = jnp.where((lane // (2**bit)) % 2 == 1, frequency * factor, frequency)
    position = jnp.zeros((8, 128), F32)
    for r in range(8):
        position = jnp.where(row == r, lengths[r].astype(F32), position)
    angles = position * frequency
    cosine = jnp.cos(angles)
    sine = jnp.sin(angles)
    sine = jnp.where(lax.broadcasted_iota(jnp.int32, (8, 128), 1) < 64, -sine, sine)
    head = jnp.full((1, 256), tp, jnp.int32).astype(F32)
    decay = 1.0 - jnp.exp2(-5.0 - 10.0 * head / (HEADS - 1))

    loads["tok"].wait()
    pl.semaphore_wait(barrier, 30)

    wait_tokens = exchange(TOK, "tp", lambda peer: tok_own, tok_all)
    tok_all[tp] = tok_own[...]
    loads["gain1"].wait()
    for name in ("wq", "wk", "wv", "wg"):
        loads[name].wait()
    wait_tokens()

    def squares_and_normed(blocks, gain, own, everyone, phase):
        wide = blocks[...].reshape(256, BATCH).astype(F32)
        own[...] = jnp.sum(wide * wide, axis=0, keepdims=True)
        wait = exchange(phase, "kv", lambda peer: own, everyone)
        everyone[kv] = own[...]
        return (wide.T * gain[...]).astype(BF16), wait

    def inverse_rms(everyone):
        total = jnp.sum(everyone[...], axis=0)
        total = jnp.broadcast_to(total, (8, BATCH))
        mine = lax.broadcasted_iota(jnp.int32, (8, BATCH), 1) == (
            kv * 8 + lax.broadcasted_iota(jnp.int32, (8, BATCH), 0)
        )
        mean = jnp.sum(jnp.where(mine, total, 0.0), axis=1, keepdims=True) / D
        return lax.rsqrt(mean + 1e-06)

    normed, wait_squares = squares_and_normed(tok_all, gain1, sq_own, sq_all, SQ1)
    part = jnp.dot(normed, w_in[...], preferred_element_type=F32)
    proj_own[...] = part.reshape(16, 8, 768).astype(BF16)
    wait_proj = exchange(QKVG, "kv", lambda peer: proj_own.at[peer], proj_all)
    proj_all[kv] = proj_own[kv]

    loads["wo"].wait()
    w_out_t[...] = w_out[...].T
    loads["state"].wait()

    wait_squares()
    wait_proj()
    owned = jnp.sum(proj_all[...].astype(F32), axis=0) * inverse_rms(sq_all)

    def rotary(v):
        return v * cosine + pltpu.roll(v, 64, 1) * sine

    query = rotary(owned[:, :128]).astype(BF16).astype(F32)
    key = (rotary(owned[:, 128:256]) * QK ** (-0.5)).astype(BF16).astype(F32)
    value = owned[:, 256:512].astype(BF16).astype(F32)
    gate = owned[:, 512:768]

    query_t = query.T
    key_t = key.T
    crossed = jnp.sum(query * key, axis=1, keepdims=True)
    from_state = jnp.concatenate(
        [
            jnp.sum(query_t[:, s : s + 1] * state[s], axis=0, keepdims=True)
            for s in range(8)
        ],
        axis=0,
    )
    retained = decay * from_state + crossed * value
    normalized = retained * lax.rsqrt(
        jnp.mean(retained * retained, axis=1, keepdims=True) + 1e-06
    )
    merged_own[...] = (normalized * (gate / (1.0 + jnp.exp(-gate)))).astype(BF16)
    wait_merged = exchange(MERGED, "kv", lambda peer: merged_own, merged_all)
    merged_all[kv] = merged_own[...]

    for s in range(8):
        new_state[s] = decay * state[s] + key_t[:, s : s + 1] * value[s : s + 1, :]
    store_state = pltpu.make_async_copy(new_state, new_state_hbm, store_sem)
    store_state.start()

    wait_merged()

    def sums_over_tp(phase, weights_t, rows, own, everyone):
        part_t = lax.dot_general(
            weights_t, rows, (((1,), (1,)), ((), ())), preferred_element_type=F32
        )
        own[...] = part_t.reshape(16, 16, BATCH).astype(BF16)
        wait = exchange(phase, "tp", lambda peer: own.at[peer], everyone)
        everyone[tp] = own[tp]
        return wait

    rows = merged_all[...].astype(F32).reshape(BATCH, VD).astype(BF16)
    wait_mixed = sums_over_tp(MIXED, w_out_t[...], rows, mixed_own, mixed_all)
    loads["fd"].wait()
    w_down_t[:, pl.ds(640, 128)] = jnp.zeros((256, 128), BF16)
    w_down_t[:, pl.ds(0, 704)] = w_down[...].T
    loads["gain2"].wait()
    loads["fg"].wait()
    loads["fu"].wait()
    wait_mixed()
    mixed = jnp.sum(mixed_all[...].astype(F32), axis=0)
    resid_own[...] = (tok_own[...].astype(F32) + mixed).astype(BF16)
    wait_resid = exchange(RESID, "tp", lambda peer: resid_own, resid_all)
    resid_all[tp] = resid_own[...]
    wait_resid()

    normed2, wait_squares2 = squares_and_normed(resid_all, gain2, sq2_own, sq2_all, SQ2)
    part2 = lax.dot_general(
        normed2, w_ff[...], (((1,), (1,)), ((), ())), preferred_element_type=F32
    )
    ffn_own[...] = part2.reshape(16, 8, 1408).astype(BF16)
    wait_ffn = exchange(FFN, "kv", lambda peer: ffn_own.at[peer], ffn_all)
    ffn_all[kv] = ffn_own[kv]
    wait_squares2()
    wait_ffn()
    summed = jnp.sum(ffn_all[...].astype(F32), axis=0) * inverse_rms(sq2_all)
    gate_ff = summed[:, :704]
    up_ff = summed[:, 704:]
    hidden = gate_ff / (1.0 + jnp.exp(-gate_ff)) * up_ff
    hidden_own[...] = jnp.concatenate([hidden, jnp.zeros((8, 64), F32)], axis=1).astype(BF16)
    wait_hidden = exchange(HIDDEN, "kv", lambda peer: hidden_own, hidden_all)
    hidden_all[kv] = hidden_own[...]
    wait_hidden()

    rows2 = hidden_all[...].astype(F32).reshape(BATCH, 768).astype(BF16)
    wait_down = sums_over_tp(DOWN, w_down_t[...], rows2, down_own, down_all)
    for wait_send in pending[:-1]:
        wait_send()
    store_state.wait()
    wait_down()
    down = jnp.sum(down_all[...].astype(F32), axis=0)
    out_ref[...] = (resid_own[...].astype(F32) + down).astype(BF16)
    pending[-1]()


def on_device(
    tokens,
    lengths,
    retention_state,
    mixer_gain,
    query_weight,
    key_weight,
    value_weight,
    gate_weight,
    output_weight,
    channel_gain,
    ffn_gate,
    ffn_up,
    ffn_down,
):
    vmem = pltpu.VMEM
    out_t, new_state = pl.pallas_call(
        kernel,
        out_shape=(
            jax.ShapeDtypeStruct((16, BATCH), BF16),
            jax.ShapeDtypeStruct((8, QK, VD), F32),
        ),
        in_specs=[pl.BlockSpec(memory_space=pl.ANY)]
        + [pl.BlockSpec(memory_space=pltpu.SMEM)]
        + [pl.BlockSpec(memory_space=pl.ANY)] * 11,
        out_specs=(
            pl.BlockSpec(memory_space=vmem),
            pl.BlockSpec(memory_space=pl.ANY),
        ),
        scratch_shapes=[
            vmem((16, BATCH), BF16),
            vmem((1, 256), F32),
            vmem((1, 256), F32),
            vmem((256, 768), BF16),
            vmem((256, 256), BF16),
            vmem((256, 256), BF16),
            vmem((1408, 256), BF16),
            vmem((704, 256), BF16),
            vmem((256, 768), BF16),
            vmem((8, QK, VD), F32),
            vmem((8, QK, VD), F32),
            vmem((16, 16, BATCH), BF16),
            vmem((1, BATCH), F32),
            vmem((16, 1, BATCH), F32),
            vmem((16, 8, 768), BF16),
            vmem((16, 8, 768), BF16),
            vmem((8, VD), BF16),
            vmem((16, 8, VD), BF16),
            vmem((16, 16, BATCH), BF16),
            vmem((16, 16, BATCH), BF16),
            vmem((16, BATCH), BF16),
            vmem((16, 16, BATCH), BF16),
            vmem((1, BATCH), F32),
            vmem((16, 1, BATCH), F32),
            vmem((16, 8, 1408), BF16),
            vmem((16, 8, 1408), BF16),
            vmem((8, 768), BF16),
            vmem((16, 8, 768), BF16),
            vmem((16, 16, BATCH), BF16),
            vmem((16, 16, BATCH), BF16),
            pltpu.SemaphoreType.DMA((N_WEIGHT_COPIES,)),
            pltpu.SemaphoreType.DMA,
            pltpu.SemaphoreType.DMA((10, 16)),
            pltpu.SemaphoreType.DMA((10, 16)),
        ],
        compiler_params=pltpu.CompilerParams(
            collective_id=0, has_side_effects=True
        ),
    )(
        tokens.T,
        lengths,
        retention_state.reshape(8, QK, VD),
        mixer_gain.reshape(1, 256),
        query_weight,
        key_weight,
        value_weight,
        gate_weight,
        output_weight,
        channel_gain.reshape(1, 256),
        ffn_gate.T,
        ffn_up.T,
        ffn_down,
    )
    return out_t.T, new_state.reshape(8, 1, QK, VD)


def solution(mesh):
    in_specs = (
        P(None, ("kv", "tp")),
        P("kv"),
        P("kv", "tp", None, None),
        P("kv"),
        P("kv", "tp"),
        P("kv", "tp"),
        P("kv", "tp"),
        P("kv", "tp"),
        P("tp", "kv"),
        P("kv"),
        P("kv", "tp"),
        P("kv", "tp"),
        P("tp", "kv"),
    )
    out_specs = (P(None, ("kv", "tp")), P("kv", "tp", None, None))
    return jax.shard_map(
        on_device, mesh=mesh, in_specs=in_specs, out_specs=out_specs, check_vma=False
    )
```

time: 127 us -> 61.3 us (0.48)
  blocking collectives: 96.8 us -> 0 us
  Pallas kernels: 0 us -> 56.9 us
  matrix products: 8.66 us -> 0 us
  waiting for transfers between devices: 7.25 us -> 0 us
  starting transfers between devices: 6.75 us -> 0 us
  other arithmetic: 1.99 us -> 0 us
    all_to_all x5 -> x0, blocking collectives: 60.1 us -> none  [the longest x3 40.5 us: sent_and_summed(): lax.all_to_all(blocks, axis, split_axis=0, concat_axis=0, tiled=True)]
    pallas_call x0 -> x1, Pallas kernels: none -> 56.9 us  [on_device(): pl.pallas_call(kernel, out_shape=(jax.ShapeDtypeStruct((16, BATCH), BF16)...]
    all_gather x2 -> x0, blocking collectives: 36.7 us -> none  [gathered_rows(): return lax.all_gather(columns, 'tp', axis=1, tiled=True)]
    dot_general x9 -> x0, matrix products: 8.66 us -> none  [the longest x1 1.83 us: on_device(): jnp.dot(normed, value_weight, preferred_element_type=jnp.float32)]
    all_to_all x1 -> x0, waiting for transfers between devices: 7.25 us -> none  [sent_and_summed(): lax.all_to_all(blocks, axis, split_axis=0, concat_axis=0, tiled=True)]
    all_to_all x1 -> x0, starting transfers between devices: 6.75 us -> none  [sent_and_summed(): lax.all_to_all(blocks, axis, split_axis=0, concat_axis=0, tiled=True)]
    unnamed x18 -> x4, local copies, waits for them, and re-layouts: 2.27 us -> 3.53 us
  transfers between devices with their start and end apart: 1 -> 0, of which waited for: 1 -> 0; matrix products, arithmetic and copies ran while one was open for 0% -> 0% of each run, Pallas kernels for 0% -> 0%
where the time goes in v1:
time: 61.3 us; the launch traced here: 61.1 us
  Pallas kernels  56.9 us (93%)
  local copies, waits for them, and re-layouts  3.53 us (6%)
  between operations  0.65 us (1%)
    pallas_call x1, Pallas kernels, on_device(): pl.pallas_call(kernel, out_shape=(jax.ShapeDtypeStruct((16, BATCH), BF16)...  56.9 us
    unnamed x4, local copies, waits for them, and re-layouts  3.53 us

profile of v1, /device:TPU:1, one launch (start us, length us, event | category | flops | bytes accessed | tf_op | source)
XLA Modules:
  0.0 61.1 jit_solution(14528102312353703496)
XLA Ops:
  0.6 56.9 %shard_map.140 = (bf16[16,128]{1,0:T(8,128)(2,1)}, f32[8,128,256]{2,1,0:T(8,128)}) custom-call(bf16[16,128]{1,0:T(8,128)(2,1)} %bitcast.14, s32[8]{0:T(128)} %lengths.1, f32[8,128,256]{2,1,0:T(8,128)} %bitcast.10, f32[1,256]{1,0:T(1,128)} %bitcast.16, bf16[256,128]{1,0:T(8,128)(2,1)} %wq_hbm.1, bf16[256,128]{1,0:T(8,128)(2,1)} %wk_hbm.1, ...), custom_call_target="tpu_custom_call" | custom-call | tf_op jit(solution)/shard_map/pallas_call | solution.py:315
  57.5 0.0 copy-start
  57.6 0.7 %copy-done = bf16[16,128]{1,0:T(8,128)(2,1)S(1)} copy-done((bf16[16,128]{1,0:T(8,128)(2,1)S(1)}, bf16[16,128]{1,0:T(8,128)(2,1)}, u32[]{:S(2)}) %copy-start) | copy-done | bytes 4120
  58.2 0.6 copy.18
  58.8 2.3 %copy.19 = f32[8,1,128,256]{3,2,1,0:T(8,128)} copy(f32[8,1,128,256]{3,2,1,0:T(8,128)} %bitcast.11) | data formatting | bytes 2097152
Async XLA Ops:
  57.5 0.7 %copy-start = (bf16[16,128]{1,0:T(8,128)(2,1)S(1)}, bf16[16,128]{1,0:T(8,128)(2,1)}, u32[]{:S(2)}) copy-start(bf16[16,128]{1,0:T(8,128)(2,1)} %get-tuple-element.4) | copy-start | bytes 12292
